TPU v7x, 32 devices: a whole 2x2x4 slice. The times are simulated.
32 devices in a mesh: grp: 2 (over x), ep: 8 (over z, y), tp: 2 (over core).
Axes of the slice: x: 2, y: 2, z: 4, core: 2. Of those that a mesh axis runs over, the one named last changes fastest.
Arguments:
- tokens: bfloat16 [2304, 2048], P(('grp', 'ep')), parts along dimension 0, may hold values from -6 to 6
- norm_gain: bfloat16 [2048], replicated, may hold values from 0.099609375 to 1.8984375
- chosen_rows: int32 [16, 144], P('grp', 'ep'), parts along dimension 0, may hold values from 0 to 1151, as said below
- route_weights: float32 [16, 144], P('grp', 'ep'), parts along dimension 0, may hold values from 0.2 to 1
- gate_weight: bfloat16 [8, 2048, 1536], P('ep', None, 'tp'), may hold values from -0.125 to 0.125
- up_weight: bfloat16 [8, 2048, 1536], P('ep', None, 'tp'), may hold values from -0.125 to 0.125
- down_weight: bfloat16 [8, 1536, 2048], P('ep', 'tp'), may hold values from -0.15625 to 0.15625
Outputs:
- mixed: bfloat16 [2304, 2048], P(('grp', 'ep', 'tp')), parts along dimension 0
There are 2 independent parts, one for each index of `grp`. A program takes and returns all parts, laid end to end along the dimension named above; an argument that names none is the same for every part. Nothing has to cross between parts.
Inputs may be any that keep to these rules, and one draw needn't show every extreme that they name: `chosen_rows`: the columns come in blocks of 18, one block for each index of ep's 144 tokens in order. In every row the first half of a block names distinct tokens of the first half of that block's tokens, and its second half distinct tokens of the second half.
All inputs are finite; a program needn't handle non-finite values.
Results may differ from a plain program's by a relative error of at most 0.01.
Values may be sent and summed in bfloat16 or wider, within the bound.
A program may use at most 128 MiB of HBM per device.

v0:
```python
import functools

import jax
import jax.numpy as jnp
from jax import lax
from jax.experimental import pallas as pl
from jax.experimental.pallas import tpu as pltpu
from jax.sharding import PartitionSpec as P

MESH = pl.DeviceIdType.MESH
LANES = 128
SUB = 8
GROUP = 8
VMEM_BYTES = 67043328


def loop(count, body):
    if count == 1:
        body(0)
    else:
        lax.fori_loop(0, count, lambda i, carry: (body(i), carry)[1], 0)


def group_sizes(half):
    return [half // 2, half - half // 2]


def kernel(
    n,
    tokens,
    gain_h,
    chosen_h,
    route_h,
    gate_w,
    up_w,
    down_w,
    mixed,
    tok,
    gain,
    chosen,
    route,
    wg,
    wu,
    wd,
    normed,
    out_x,
    in_x,
    sib_x,
    flat,
    x_cols,
    hidden,
    p_send,
    p_recv,
    p_own,
    c_send,
    c_recv,
    g_rows,
    w_rows,
    r_cols,
    load_sem,
    d_send,
    d_recv,
    f_send,
    f_recv,
    q_send,
    q_recv,
    b_send,
    b_recv,
):
    half_rows, width = tok.shape
    experts, slots = chosen.shape
    half = slots // 2
    sizes = group_sizes(half)
    starts = [sum(sizes[:j]) for j in range(len(sizes))]
    blocks = experts // GROUP
    pieces = width // LANES
    cols = width // 2
    me = lax.axis_index("ep")
    core = lax.axis_index("tp")
    sib = {"tp": 1 - core}

    def peer(i):
        return lax.rem(me + i, n)

    barrier = pltpu.get_barrier_semaphore()
    pl.semaphore_signal(barrier, inc=1, device_id=sib, device_id_type=MESH)
    lax.fori_loop(
        1,
        n,
        lambda i, c: (
            pl.semaphore_signal(barrier, inc=1, device_id={"ep": peer(i)}, device_id_type=MESH),
            c,
        )[1],
        0,
    )
    base = pl.multiple_of(core * half_rows, 8)
    load_tok = pltpu.make_async_copy(tokens.at[pl.ds(base, half_rows)], tok, load_sem.at[0])
    load_tok.start()
    small = [
        pltpu.make_async_copy(src, dst, load_sem.at[i + 4])
        for i, (src, dst) in enumerate(((gain_h, gain), (chosen_h, chosen), (route_h, route)))
    ]
    for load in small:
        load.start()
    loads = [
        pltpu.make_async_copy(src.at[0], dst, load_sem.at[i + 1])
        for i, (src, dst) in enumerate(((gate_w, wg), (up_w, wu), (down_w, wd)))
    ]
    for load in small:
        load.wait()
    first = me * (2 * half_rows) + core * half_rows
    picked = (chosen[...] - first).astype(jnp.float32).T
    weight = route[...].T
    lane = lax.broadcasted_iota(jnp.int32, (half, half_rows), 1).astype(jnp.float32)
    for e in range(experts):
        pair = [picked[h * half : (h + 1) * half, e : e + 1] for h in range(2)]
        row = jnp.where(core == 0, pair[0], pair[1])
        pair = [weight[h * half : (h + 1) * half, e : e + 1] for h in range(2)]
        share = jnp.where(core == 0, pair[0], pair[1])
        here = lane == row
        for j, size in enumerate(sizes):
            here_j = slice(starts[j], starts[j] + size)
            at = slice(experts * starts[j] + e * size, experts * starts[j] + (e + 1) * size)
            g_rows[at, :] = jnp.where(here, 1.0, 0.0)[here_j]
            w_rows[at, :] = jnp.where(here, share, 0.0)[here_j]

    load_tok.wait()
    for load in loads:
        load.start()

    g = gain[...].astype(jnp.float32).reshape(1, width)
    values = tok[...].astype(jnp.float32)
    scale = lax.rsqrt(jnp.mean(values * values, axis=-1, keepdims=True) + 1e-06)
    normed[...] = (values * scale * g).astype(jnp.bfloat16)

    def rows_of(j, b):
        block = GROUP * sizes[j]
        at = b * block
        return pl.ds(at if isinstance(b, int) else pl.multiple_of(at, 8), block)

    def total_rows(j, b):
        block = GROUP * sizes[j]
        at = experts * starts[j] + b * block
        return pl.ds(at if isinstance(b, int) else pl.multiple_of(at, 8), block)

    def pack(value, ref, j, b):
        block = GROUP * sizes[j]
        for s in range(pieces):
            flat[pl.ds(s, block, stride=pieces), :] = value[:, s * LANES : (s + 1) * LANES]
        packed = flat[: block * pieces, :].reshape(block, pieces, LANES)
        ref[j, rows_of(j, b)] = packed.astype(jnp.bfloat16)

    def gather(j):
        def one(b):
            hot = g_rows[total_rows(j, b), :].astype(jnp.bfloat16)
            got = jnp.dot(hot, normed[...], preferred_element_type=jnp.float32)
            pack(got, out_x, j, b)

        loop(blocks, one)

    def mine(ref, j, e):
        return ref.at[j, pl.ds(e * sizes[j], sizes[j])]

    def exchange(src, dst, j, send_sem, recv_sem):
        def one(i, c):
            e = peer(i)
            pltpu.make_async_remote_copy(
                src_ref=mine(src, j, e),
                dst_ref=mine(dst, j, me),
                send_sem=send_sem.at[j],
                recv_sem=recv_sem.at[j],
                device_id={"ep": e},
                device_id_type=MESH,
            ).start()
            return c

        lax.fori_loop(1, n, one, 0)
        for r in range(sizes[j]):
            dst[j, me * sizes[j] + r] = src[j, me * sizes[j] + r]

    def all_of(src, dst, j, send_sem, recv_sem):
        part = pl.ds(0, (n - 1) * sizes[j])
        return pltpu.make_async_remote_copy(
            src_ref=src.at[j, part],
            dst_ref=dst.at[j, part],
            send_sem=send_sem.at[j],
            recv_sem=recv_sem.at[j],
            device_id=sib,
            device_id_type=MESH,
        )

    def forward(j):
        part = pl.ds(0, n * sizes[j])
        return pltpu.make_async_remote_copy(
            src_ref=in_x.at[j, part],
            dst_ref=sib_x.at[j, part],
            send_sem=f_send.at[j],
            recv_sem=f_recv.at[j],
            device_id=sib,
            device_id_type=MESH,
        )

    def swap(j, k):
        part = pl.ds(0, n * sizes[j])
        return pltpu.make_async_remote_copy(
            src_ref=p_send.at[j, k, part],
            dst_ref=p_recv.at[j, k, part],
            send_sem=q_send.at[2 * j + k],
            recv_sem=q_recv.at[2 * j + k],
            device_id=sib,
            device_id_type=MESH,
        )

    groups = range(len(sizes))
    gather(0)
    pl.semaphore_wait(barrier, n)
    exchange(out_x, in_x, 0, d_send, d_recv)
    for j in groups[1:]:
        gather(j)
        exchange(out_x, in_x, j, d_send, d_recv)

    def arrive(j):
        all_of(out_x, in_x, j, d_send, d_recv).wait_recv()
        forward(j).start()

    def compute(j):
        block = GROUP * sizes[j]

        def project(b):
            for h, ref in enumerate((in_x, sib_x)):
                got = ref[j, rows_of(j, b)].astype(jnp.float32)
                flat[pl.ds(h * block * pieces, block * pieces), :] = got.reshape(
                    block * pieces, LANES
                )
            for s in range(pieces):
                x_cols[: 2 * block, s * LANES : (s + 1) * LANES] = flat[
                    pl.ds(s, 2 * block, stride=pieces), :
                ].astype(jnp.bfloat16)
            x = x_cols[: 2 * block, :]
            gate = jnp.dot(x, wg[...], preferred_element_type=jnp.float32)
            up = jnp.dot(x, wu[...], preferred_element_type=jnp.float32)
            act = (gate / (1.0 + jnp.exp(-gate)) * up).astype(jnp.bfloat16)
            hidden[b, : 2 * block, :] = act

        loop(blocks, project)
        if j == 0:
            loads[2].wait()
        for k in range(2):

            def down(b):
                part = jnp.dot(
                    hidden[b, : 2 * block, :],
                    wd[:, k * cols : (k + 1) * cols],
                    preferred_element_type=jnp.float32,
                )
                p_own[j, k, rows_of(j, b)] = part[:block].astype(jnp.bfloat16)
                p_send[j, k, rows_of(j, b)] = part[block:].astype(jnp.bfloat16)

            loop(blocks, down)
            swap(j, k).start()

    def give(j):
        for k in range(2):
            swap(j, k).wait_recv()

        def combine(b):
            both = [
                p_own[j, k, rows_of(j, b)].astype(jnp.float32)
                + p_recv[j, k, rows_of(j, b)].astype(jnp.float32)
                for k in range(2)
            ]
            pack(jnp.concatenate(both, axis=1), c_send, j, b)

        loop(blocks, combine)
        exchange(c_send, c_recv, j, b_send, b_recv)

    arrive(0)
    for load in loads[:2]:
        load.wait()
    for j in groups:
        forward(j).wait_recv()
        compute(j)
        if j + 1 < len(sizes):
            arrive(j + 1)
        give(j)

    spread = w_rows[...].T
    high = spread.astype(jnp.bfloat16)
    low = (spread - high.astype(jnp.float32)).astype(jnp.bfloat16)
    for j in groups:
        all_of(c_send, c_recv, j, b_send, b_recv).wait_recv()
        block = GROUP * sizes[j]

        def unpack(b):
            got = c_recv[j, rows_of(j, b)].astype(jnp.float32)
            flat[: block * pieces, :] = got.reshape(block * pieces, LANES)
            for s in range(pieces):
                r_cols[total_rows(j, b), s * LANES : (s + 1) * LANES] = flat[
                    pl.ds(s, block, stride=pieces), :
                ]

        loop(blocks, unpack)
    for k in range(2):
        part = slice(k * cols, (k + 1) * cols)
        res = r_cols[:, part].astype(jnp.bfloat16)
        total = jnp.dot(high, res, preferred_element_type=jnp.float32)
        total = total + jnp.dot(low, res, preferred_element_type=jnp.float32)
        mixed[:, part] = total.astype(jnp.bfloat16)

    for j in groups:
        all_of(out_x, in_x, j, d_send, d_recv).wait_send()
        forward(j).wait_send()
        for k in range(2):
            swap(j, k).wait_send()
        all_of(c_send, c_recv, j, b_send, b_recv).wait_send()


def local(n, tokens, norm_gain, chosen_rows, route_weights, gate_weight, up_weight, down_weight):
    tok_rows, width = tokens.shape
    half_rows = tok_rows // 2
    experts, slots = chosen_rows.shape
    half = slots // 2
    rows = experts * half
    sizes = group_sizes(half)
    top = max(sizes)
    block = GROUP * top
    pieces = width // LANES
    ff = gate_weight.shape[2]
    bf16, f32 = jnp.bfloat16, jnp.float32
    packed = pltpu.VMEM((len(sizes), experts * top, pieces, LANES), bf16)
    partial = pltpu.VMEM((len(sizes), 2, experts * top, width // 2), bf16)
    vmem = pl.BlockSpec(memory_space=pltpu.VMEM)
    hbm = pl.BlockSpec(memory_space=pltpu.HBM)
    scratch = [
        pltpu.VMEM((half_rows, width), bf16),
        pltpu.VMEM(norm_gain.shape, norm_gain.dtype),
        pltpu.VMEM(chosen_rows.shape, chosen_rows.dtype),
        pltpu.VMEM(route_weights.shape, route_weights.dtype),
        pltpu.VMEM(gate_weight.shape[1:], bf16),
        pltpu.VMEM(up_weight.shape[1:], bf16),
        pltpu.VMEM(down_weight.shape[1:], bf16),
        pltpu.VMEM((half_rows, width), bf16),
        packed,
        packed,
        packed,
        pltpu.VMEM((2 * block * pieces, LANES), f32),
        pltpu.VMEM((2 * block, width), bf16),
        pltpu.VMEM((experts // GROUP, 2 * block, ff), bf16),
        partial,
        partial,
        partial,
        packed,
        packed,
        pltpu.VMEM((rows, half_rows), f32),
        pltpu.VMEM((rows, half_rows), f32),
        pltpu.VMEM((rows, width), f32),
    ]
    limit = VMEM_BYTES - half_rows * width * 2
    return pl.pallas_call(
        functools.partial(kernel, n),
        out_shape=pltpu.VMEM((half_rows, width), bf16),
        in_specs=[hbm] * 7,
        out_specs=vmem,
        scratch_shapes=scratch
        + [pltpu.SemaphoreType.DMA((7,))]
        + [pltpu.SemaphoreType.DMA((2 * len(sizes),))] * 8,
        compiler_params=pltpu.CompilerParams(
            collective_id=0, has_side_effects=True, vmem_limit_bytes=limit
        ),
    )(
        tokens,
        norm_gain,
        chosen_rows,
        route_weights,
        gate_weight,
        up_weight,
        down_weight,
    )


def solution(mesh):
    return jax.shard_map(
        functools.partial(local, mesh.shape["ep"]),
        mesh=mesh,
        in_specs=(
            P(("grp", "ep"), None),
            P(),
            P("grp", "ep"),
            P("grp", "ep"),
            P("ep", None, "tp"),
            P("ep", None, "tp"),
            P("ep", "tp", None),
        ),
        out_specs=P(("grp", "ep", "tp"), None),
        check_vma=False,
    )
```

profile of v0, /device:TPU:0, one launch (start us, length us, event | category | flops | bytes accessed | tf_op | source)
XLA Modules:
  0.0 24.6 jit_solution(7999714500178998200)
XLA Ops:
  0.0 23.9 %shard_map.73 = bf16[72,2048]{1,0:T(8,128)(2,1)S(1)} custom-call(bf16[144,2048]{1,0:T(8,128)(2,1)} %tokens.1, bf16[2048]{0:T(1024)(128)(2,1)} %gain_h.1, s32[8,18]{1,0:T(8,128)} %chosen_h.1, f32[8,18]{1,0:T(8,128)} %route_h.1, bf16[1,2048,768]{2,1,0:T(8,128)(2,1)} %gate_w.1, bf16[1,2048,768]{2,1,0:T(8,128)(2,1)} %up_w.1, bf16[1,768,2048]{2,1,0:T(8,128)(2,1)} %down_w.1), custom_call_target="tpu_custom_call" | custom-call | tf_op jit(solution)/shard_map/pallas_call | solution.py:359
  23.9 0.7 %copy.9 = bf16[72,2048]{1,0:T(8,128)(2,1)} copy(bf16[72,2048]{1,0:T(8,128)(2,1)S(1)} %shard_map.73) | data formatting | bytes 589824
where the time goes:
time: 24.9 us; the launch traced here: 24.6 us
  Pallas kernels  23.9 us (96%)
  local copies, waits for them, and re-layouts  0.72 us (3%)
    pallas_call x1, Pallas kernels, local(): pl.pallas_call(functools.partial(kernel, n), out_shape=pltpu.VMEM((half_r...  23.9 us
    unnamed x1, local copies, waits for them, and re-layouts  0.72 us

commit v1 on v0

v1 whole, which is shorter than its diff:
```python
import functools

import jax
import jax.numpy as jnp
from jax import lax
from jax.experimental import pallas as pl
from jax.experimental.pallas import tpu as pltpu
from jax.sharding import PartitionSpec as P

MESH = pl.DeviceIdType.MESH
LANES = 128
PARTS = 2
CUTS = 1
TILE = 256
VMEM_BYTES = 67043328


phase = jax.named_scope


def loop(count, body):
    if count == 1:
        body(0)
    else:
        lax.fori_loop(0, count, lambda i, carry: (body(i), carry)[1], 0)


def each(low, high, body):
    lax.fori_loop(low, high, lambda i, carry: (body(i), carry)[1], 0)


def group_sizes(half):
    base = half // PARTS
    sizes = [base + (1 if i >= PARTS - half % PARTS else 0) for i in range(PARTS)]
    return [s for s in sizes if s]


def round_up(a, b):
    return (a + b - 1) // b * b


def kernel(
    n,
    tokens,
    gain_h,
    chosen_h,
    route_h,
    gate_w,
    up_w,
    down_w,
    mixed,
    tok,
    gain,
    chosen,
    route,
    wgu,
    wd,
    out_x,
    in_x,
    sib_x,
    flat,
    x_cols,
    hidden,
    p_send,
    p_recv,
    p_own,
    c_send,
    c_recv,
    g_rows,
    w_rows,
    spread,
    r_cols,
    load_sem,
    d_send,
    d_recv,
    f_send,
    f_recv,
    q_send,
    q_recv,
    b_send,
    b_recv,
    ready,
):
    tok_rows, width = tok.shape
    half_rows = tok_rows // 2
    experts, slots = chosen.shape
    half = slots // 2
    sizes = group_sizes(half)
    starts = [sum(sizes[:j]) for j in range(len(sizes))]
    chunks = range(len(sizes))
    side = n // 2
    quarter = n // 4
    bunch = min(side, 4)
    blocks = side // bunch
    pad = x_cols.shape[1] // 2
    pieces = width // LANES
    cols = width // CUTS
    f32, bf16 = jnp.float32, jnp.bfloat16
    me = lax.axis_index("ep")
    core = lax.axis_index("tp")
    sib = {"tp": 1 - core}
    upper = lax.div(me, side)
    spot = me - upper * side
    far_half = upper + core - 2 * upper * core
    base = far_half * side
    lower_far = core * (1 - upper)
    last_far = core * lax.div(me, 3 * quarter)

    barrier = pltpu.get_barrier_semaphore()

    def greet(semaphore, target):
        pl.semaphore_signal(semaphore, inc=1, device_id=target, device_id_type=MESH)

    greet(barrier, sib)
    near_first = 1 - core
    each(
        near_first,
        side * (1 - last_far),
        lambda i: greet(barrier, {"ep": base + lax.rem(spot * near_first + i, side)}),
    )
    load_tok = pltpu.make_async_copy(tokens, tok, load_sem.at[0])
    small = [
        pltpu.make_async_copy(src, dst, load_sem.at[i + 4])
        for i, (src, dst) in enumerate(((gain_h, gain), (chosen_h, chosen), (route_h, route)))
    ]
    small[1].start()
    load_tok.start()
    small[0].start()
    small[2].start()
    ff = wd.shape[0]
    loads = [
        pltpu.make_async_copy(src.at[0], dst, load_sem.at[i + 1])
        for i, (src, dst) in enumerate(
            (
                (gate_w, wgu.at[:, pl.ds(0, ff)]),
                (up_w, wgu.at[:, pl.ds(ff, ff)]),
                (down_w, wd),
            )
        )
    ]

    @pl.when(last_far == 1)
    def _():
        pl.semaphore_wait(barrier, 1 + side)
        each(0, side, lambda i: greet(ready, {"ep": i}))

    with phase("load"):
        small[1].wait()
    picked = (chosen[...] - me * tok_rows).astype(f32)
    mine_rows = jnp.where(far_half == 1, picked[side:], picked[:side])

    def hot_rows(j):
        size = sizes[j]
        rows = side * 2 * size
        row = lax.broadcasted_iota(jnp.int32, (rows, slots), 0)
        lane = lax.broadcasted_iota(jnp.int32, (rows, slots), 1)
        value = jnp.zeros((rows, slots), f32)
        want = jnp.zeros((rows, slots), jnp.int32)
        for k in range(side):
            for h in range(2):
                at = (2 * k + h) * size
                here = row >= at
                if h == 0:
                    value = jnp.where(here, mine_rows[k : k + 1, :], value)
                want = jnp.where(here, row + (h * half + starts[j] - at), want)
        index = jnp.sum(jnp.where(lane == want, value, 0.0), axis=-1, keepdims=True)
        token = lax.broadcasted_iota(jnp.int32, (rows, tok_rows), 1).astype(f32)
        return jnp.where(token == index, 1.0, 0.0)

    def block_rows(b, count):
        at = b * count
        return pl.ds(at if isinstance(b, int) else pl.multiple_of(at, count), count)

    def pack(value, ref, j, b):
        count = value.shape[0]
        for s in range(pieces):
            flat[pl.ds(s, count, stride=pieces), :] = value[:, s * LANES : (s + 1) * LANES]
        packed = flat[: count * pieces, :].reshape(count, pieces, LANES)
        ref[j, block_rows(b, count)] = packed.astype(bf16)

    def gather(j):
        count = bunch * 2 * sizes[j]
        with phase("hot"):
            g_rows[: blocks * count, :] = hot_rows(j)
        if j == 0:
            with phase("tok"):
                load_tok.wait()
                small[0].wait()
            for load in loads:
                load.start()

        def one(b):
            hot = g_rows[block_rows(b, count), :].astype(bf16)
            with phase("norm"):
                got = jnp.dot(hot, tok[...], preferred_element_type=f32)
                scale = lax.rsqrt(jnp.mean(got * got, axis=-1, keepdims=True) + 1e-06)
                got = got * scale * gain[...].astype(f32).reshape(1, width)
            with phase("pack"):
                pack(got, out_x, j, b)

        loop(blocks, one)

    def dispatch(j, low, high):
        count = 2 * sizes[j]

        def one(i):
            k = lax.rem(spot * near_first + i, side)
            pltpu.make_async_remote_copy(
                src_ref=out_x.at[j, pl.ds(k * count, count)],
                dst_ref=in_x.at[j, pl.ds(spot * count, count)],
                send_sem=d_send.at[j],
                recv_sem=d_recv.at[j],
                device_id={"ep": base + k},
                device_id_type=MESH,
            ).start()

        each(low, high, one)

    def keep_dispatch(j):
        count = 2 * sizes[j]

        @pl.when(core == 0)
        def _():
            for r in range(count):
                in_x[j, spot * count + r] = out_x[j, spot * count + r]

    def rows_copy(src, dst, j, rows, send_sem, recv_sem):
        return pltpu.make_async_remote_copy(
            src_ref=src.at[j, pl.ds(0, rows)],
            dst_ref=dst.at[j, pl.ds(0, rows)],
            send_sem=send_sem.at[j],
            recv_sem=recv_sem.at[j],
            device_id=sib,
            device_id_type=MESH,
        )

    def by_core(rows_even, rows_odd, wait):
        @pl.when(core == 0)
        def _():
            wait(rows_even)

        @pl.when(core == 1)
        def _():
            wait(rows_odd)

    def dispatched(j, sent):
        count = 2 * sizes[j]

        def wait(rows):
            copy = rows_copy(out_x, in_x, j, rows, d_send, d_recv)
            copy.wait_send() if sent else copy.wait_recv()

        by_core((side - 1) * count, side * count, wait)

    def returned(j, sent):
        def wait(rows):
            copy = rows_copy(c_recv, c_recv, j, rows, b_send, b_recv)
            copy.wait_send() if sent else copy.wait_recv()

        by_core((n - 1) * sizes[j], n * sizes[j], wait)

    def forward(j):
        return rows_copy(in_x, sib_x, j, side * 2 * sizes[j], f_send, f_recv)

    def swap(j, k):
        return pltpu.make_async_remote_copy(
            src_ref=p_send.at[j, k],
            dst_ref=p_recv.at[j, k],
            send_sem=q_send.at[CUTS * j + k],
            recv_sem=q_recv.at[CUTS * j + k],
            device_id=sib,
            device_id_type=MESH,
        )

    def give_back(j):
        size = sizes[j]

        first = near_first * spot + core * (1 - upper) * quarter

        def one(i):
            k = lax.rem(first + i, side)
            for h in range(2):
                pltpu.make_async_remote_copy(
                    src_ref=c_send.at[j, pl.ds((2 * k + h) * size, size)],
                    dst_ref=c_recv.at[j, pl.ds(me * size, size)],
                    send_sem=b_send.at[j],
                    recv_sem=b_recv.at[j],
                    device_id={"ep": base + k, "tp": h},
                    device_id_type=MESH,
                ).start()

        each(near_first, side, one)

        @pl.when(core == 0)
        def _():
            pltpu.make_async_remote_copy(
                src_ref=c_send.at[j, pl.ds((2 * spot + 1) * size, size)],
                dst_ref=c_recv.at[j, pl.ds(me * size, size)],
                send_sem=b_send.at[j],
                recv_sem=b_recv.at[j],
                device_id=sib,
                device_id_type=MESH,
            ).start()
            for r in range(size):
                c_recv[j, me * size + r] = c_send[j, 2 * spot * size + r]

    def arrive(j):
        with phase(f"arrive{j}"):
            dispatched(j, False)
            forward(j).start()

    def to_cols(ref, j, at):
        count = bunch * 2 * sizes[j]

        def one(b):
            got = ref[j, block_rows(b, count)].astype(f32)
            flat[pl.ds(0, count * pieces), :] = got.reshape(count * pieces, LANES)
            for s in range(pieces):
                x_cols[b, at : at + count, s * LANES : (s + 1) * LANES] = flat[
                    pl.ds(s, count, stride=pieces), :
                ].astype(bf16)

        loop(blocks, one)

    def project(j):
        def one(b):
            for c in range(0, ff, TILE):
                gate = jnp.dot(x_cols[b], wgu[:, c : c + TILE], preferred_element_type=f32)
                up = jnp.dot(x_cols[b], wgu[:, ff + c : ff + c + TILE], preferred_element_type=f32)
                hidden[b, :, c : c + TILE] = (gate / (1.0 + jnp.exp(-gate)) * up).astype(bf16)

        loop(blocks, one)

    def down(j):
        count = bunch * 2 * sizes[j]
        for k in range(CUTS):
            part = slice(k * cols, (k + 1) * cols)

            def one(b):
                got = jnp.dot(hidden[b], wd[:, part], preferred_element_type=f32)
                p_send[j, k, b, :count] = got[pad : pad + count].astype(bf16)
                p_own[j, k, b, :count] = got[:count].astype(bf16)

            loop(blocks, one)
            swap(j, k).start()

    def combine(j):
        count = bunch * 2 * sizes[j]

        def one(b):
            both = [
                p_own[j, k, b, :count].astype(f32) + p_recv[j, k, b, :count].astype(f32)
                for k in range(CUTS)
            ]
            pack(jnp.concatenate(both, axis=1), c_send, j, b)

        loop(blocks, one)

    def finish(j):
        with phase(f"swap{j}"):
            for k in range(CUTS):
                swap(j, k).wait_recv()
        with phase(f"combine{j}"):
            combine(j)
            give_back(j)

    for j in chunks:
        with phase(f"gather{j}"):
            gather(j)
        if j == 0:

            with phase("enter"):

                @pl.when(last_far == 0)
                def _():
                    entered = side * (1 - lower_far) + (1 + quarter) * lower_far + core * upper
                    pl.semaphore_wait(barrier, entered)

        dispatch(j, near_first, side - quarter * lower_far)
        keep_dispatch(j)

    with phase("ready"):

        @pl.when(lower_far == 1)
        def _():
            pl.semaphore_wait(ready, quarter)
            for j in chunks:
                dispatch(j, quarter, side)

    small[2].wait()
    mine = (picked - core * half_rows).T
    weight = route[...].T
    lane = lax.broadcasted_iota(jnp.int32, (half, half_rows), 1).astype(f32)
    for e in range(experts):
        pair = [mine[h * half : (h + 1) * half, e : e + 1] for h in range(2)]
        row = jnp.where(core == 0, pair[0], pair[1])
        pair = [weight[h * half : (h + 1) * half, e : e + 1] for h in range(2)]
        share = jnp.where(core == 0, pair[0], pair[1])
        here = jnp.where(lane == row, share, 0.0)
        for j, size in enumerate(sizes):
            at = experts * starts[j] + e * size
            w_rows[at : at + size, :] = here[starts[j] : starts[j] + size]
    turned = w_rows[...].T
    high = turned.astype(bf16)
    spread[:half_rows, :] = high.astype(f32)
    spread[half_rows:, :] = turned - high.astype(f32)
    x_cols[...] = jnp.zeros(x_cols.shape, bf16)

    arrive(0)
    for load in loads[:2]:
        load.wait()
    for j in chunks:
        with phase(f"cols{j}"):
            to_cols(in_x, j, 0)
        with phase(f"forward{j}"):
            forward(j).wait_recv()
        if j + 1 < len(sizes):

            @pl.when(core == 0)
            def _():
                arrive(j + 1)

        with phase(f"sib{j}"):
            to_cols(sib_x, j, pad)
        with phase(f"project{j}"):
            project(j)
        if j > 0:
            finish(j - 1)
        if j + 1 < len(sizes):

            @pl.when(core == 1)
            def _():
                arrive(j + 1)

        if j == 0:
            loads[2].wait()
        with phase(f"down{j}"):
            down(j)
    finish(len(sizes) - 1)

    for j in chunks:
        with phase(f"returned{j}"):
            returned(j, False)
        block = 8 * sizes[j]

        def unpack(b):
            got = c_recv[j, block_rows(b, block)].astype(f32)
            flat[: block * pieces, :] = got.reshape(block * pieces, LANES)
            at = experts * starts[j] + b * block
            at = at if isinstance(b, int) else pl.multiple_of(at, 8)
            for s in range(pieces):
                r_cols[pl.ds(at, block), s * LANES : (s + 1) * LANES] = flat[
                    pl.ds(s, block, stride=pieces), :
                ]

        loop(experts // 8, unpack)
    for k in range(CUTS):
        part = slice(k * cols, (k + 1) * cols)
        res = r_cols[:, part].astype(bf16)
        total = jnp.dot(spread[...].astype(bf16), res, preferred_element_type=f32)
        mixed[:, part] = (total[:half_rows] + total[half_rows:]).astype(bf16)

    for j in chunks:
        dispatched(j, True)
        forward(j).wait_send()
        for k in range(CUTS):
            swap(j, k).wait_send()
        returned(j, True)


def local(n, tokens, norm_gain, chosen_rows, route_weights, gate_weight, up_weight, down_weight):
    tok_rows, width = tokens.shape
    half_rows = tok_rows // 2
    experts, slots = chosen_rows.shape
    half = slots // 2
    rows = experts * half
    sizes = group_sizes(half)
    parts = len(sizes)
    top = max(sizes)
    side = n // 2
    bunch = min(side, 4)
    blocks = side // bunch
    block = bunch * 2 * top
    pad = round_up(block, 16)
    pieces = width // LANES
    ff = gate_weight.shape[2]
    bf16, f32 = jnp.bfloat16, jnp.float32
    packed = pltpu.VMEM((parts, n * top, pieces, LANES), bf16)
    partial = pltpu.VMEM((parts, CUTS, blocks, block, width // CUTS), bf16)
    vmem = pl.BlockSpec(memory_space=pltpu.VMEM)
    hbm = pl.BlockSpec(memory_space=pltpu.HBM)
    scratch = [
        pltpu.VMEM((tok_rows, width), bf16),
        pltpu.VMEM(norm_gain.shape, norm_gain.dtype),
        pltpu.VMEM(chosen_rows.shape, chosen_rows.dtype),
        pltpu.VMEM(route_weights.shape, route_weights.dtype),
        pltpu.VMEM((width, 2 * ff), bf16),
        pltpu.VMEM(down_weight.shape[1:], bf16),
        packed,
        packed,
        packed,
        pltpu.VMEM((max(block, 8 * top) * pieces, LANES), f32),
        pltpu.VMEM((blocks, 2 * pad, width), bf16),
        pltpu.VMEM((blocks, 2 * pad, ff), bf16),
        partial,
        partial,
        partial,
        packed,
        packed,
        pltpu.VMEM((n * top, tok_rows), f32),
        pltpu.VMEM((rows, half_rows), f32),
        pltpu.VMEM((tok_rows, rows), f32),
        pltpu.VMEM((rows, width), f32),
    ]
    limit = VMEM_BYTES - half_rows * width * 2
    return pl.pallas_call(
        functools.partial(kernel, n),
        out_shape=pltpu.VMEM((half_rows, width), bf16),
        in_specs=[hbm] * 7,
        out_specs=vmem,
        scratch_shapes=scratch
        + [pltpu.SemaphoreType.DMA((7,))]
        + [pltpu.SemaphoreType.DMA((CUTS * parts,))] * 8
        + [pltpu.SemaphoreType.REGULAR],
        compiler_params=pltpu.CompilerParams(
            collective_id=0, has_side_effects=True, vmem_limit_bytes=limit
        ),
    )(
        tokens,
        norm_gain,
        chosen_rows,
        route_weights,
        gate_weight,
        up_weight,
        down_weight,
    )


def solution(mesh):
    return jax.shard_map(
        functools.partial(local, mesh.shape["ep"]),
        mesh=mesh,
        in_specs=(
            P(("grp", "ep"), None),
            P(),
            P("grp", "ep"),
            P("grp", "ep"),
            P("ep", None, "tp"),
            P("ep", None, "tp"),
            P("ep", "tp", None),
        ),
        out_specs=P(("grp", "ep", "tp"), None),
        check_vma=False,
    )
```

time: 24.9 us -> 22.7 us (0.912)
  Pallas kernels: 23.9 us -> 21.8 us
    pallas_call x1, Pallas kernels: 23.9 us -> 21.8 us  [local(): pl.pallas_call(functools.partial(kernel, n), out_shape=pltpu.VMEM((half_r...]
where the time goes in v1:
time: 22.7 us; the launch traced here: 22.5 us
  Pallas kernels  21.8 us (96%)
  local copies, waits for them, and re-layouts  0.72 us (3%)
    pallas_call x1, Pallas kernels, local(): pl.pallas_call(functools.partial(kernel, n), out_shape=pltpu.VMEM((half_r...  21.8 us
    unnamed x1, local copies, waits for them, and re-layouts  0.72 us

profile of v1, /device:TPU:0, one launch (start us, length us, event | category | flops | bytes accessed | tf_op | source)
XLA Modules:
  0.0 22.5 jit_solution(1130088683481547294)
XLA Ops:
  0.0 21.8 %shard_map.73 = bf16[72,2048]{1,0:T(8,128)(2,1)S(1)} custom-call(bf16[144,2048]{1,0:T(8,128)(2,1)} %tokens.1, bf16[2048]{0:T(1024)(128)(2,1)} %gain_h.1, s32[8,18]{1,0:T(8,128)} %chosen_h.1, f32[8,18]{1,0:T(8,128)} %route_h.1, bf16[1,2048,768]{2,1,0:T(8,128)(2,1)} %gate_w.1, bf16[1,2048,768]{2,1,0:T(8,128)(2,1)} %up_w.1, bf16[1,768,2048]{2,1,0:T(8,128)(2,1)} %down_w.1), custom_call_target="tpu_custom_call" | custom-call | tf_op jit(solution)/shard_map/pallas_call | solution.py:516
  21.8 0.7 %copy.9 = bf16[72,2048]{1,0:T(8,128)(2,1)} copy(bf16[72,2048]{1,0:T(8,128)(2,1)S(1)} %shard_map.73) | data formatting | bytes 589824

commit v2 on v1

--- a/solution.py
+++ b/solution.py
@@ -58,6 +58,7 @@
     out_x,
     in_x,
     sib_x,
+    relay_x,
     flat,
     x_cols,
     hidden,
@@ -70,7 +71,6 @@
     w_rows,
     spread,
     r_cols,
-    load_sem,
     d_send,
     d_recv,
     f_send,
@@ -79,6 +79,9 @@
     q_recv,
     b_send,
     b_recv,
+    r_send,
+    r_recv,
+    h_send,
     ready,
 ):
     tok_rows, width = tok.shape
@@ -103,8 +106,8 @@
     spot = me - upper * side
     far_half = upper + core - 2 * upper * core
     base = far_half * side
-    lower_far = core * (1 - upper)
-    last_far = core * lax.div(me, 3 * quarter)
+    place = lax.div(me, quarter)
+    role = [core * jnp.where(place == i, 1, 0) for i in range(4)]
 
     barrier = pltpu.get_barrier_semaphore()
 
@@ -114,14 +117,23 @@
     greet(barrier, sib)
     near_first = 1 - core
     each(
-        near_first,
-        side * (1 - last_far),
+        near_first + quarter * role[2],
+        side * (1 - role[3]),
         lambda i: greet(barrier, {"ep": base + lax.rem(spot * near_first + i, side)}),
     )
-    load_tok = pltpu.make_async_copy(tokens, tok, load_sem.at[0])
+
+    @pl.when(role[1] == 1)
+    def _():
+        greet(barrier, {"ep": me - quarter})
+
+    load_tok = pltpu.make_async_copy(tokens, tok, h_send.at[0])
     small = [
-        pltpu.make_async_copy(src, dst, load_sem.at[i + 4])
-        for i, (src, dst) in enumerate(((gain_h, gain), (chosen_h, chosen), (route_h, route)))
+        pltpu.make_async_copy(src, dst, sem)
+        for src, dst, sem in (
+            (gain_h, gain, h_send.at[1]),
+            (chosen_h, chosen, b_send.at[1]),
+            (route_h, route, f_send.at[0]),
+        )
     ]
     small[1].start()
     load_tok.start()
@@ -129,20 +141,18 @@
     small[2].start()
     ff = wd.shape[0]
     loads = [
-        pltpu.make_async_copy(src.at[0], dst, load_sem.at[i + 1])
-        for i, (src, dst) in enumerate(
-            (
-                (gate_w, wgu.at[:, pl.ds(0, ff)]),
-                (up_w, wgu.at[:, pl.ds(ff, ff)]),
-                (down_w, wd),
-            )
+        pltpu.make_async_copy(src.at[0], dst, sem)
+        for src, dst, sem in (
+            (gate_w, wgu.at[:, pl.ds(0, ff)], q_send.at[0]),
+            (up_w, wgu.at[:, pl.ds(ff, ff)], q_send.at[1]),
+            (down_w, wd, b_send.at[0]),
         )
     ]
 
-    @pl.when(last_far == 1)
+    @pl.when(role[3] == 1)
     def _():
         pl.semaphore_wait(barrier, 1 + side)
-        each(0, side, lambda i: greet(ready, {"ep": i}))
+        each(quarter, side, lambda i: greet(ready, {"ep": i}))
 
     with phase("load"):
         small[1].wait()
@@ -216,6 +226,36 @@
 
         each(low, high, one)
 
+    def part_rows(j, p):
+        count = quarter * 2 * sizes[j]
+        return pl.ds(p * count, count)
+
+    def relay(j, p):
+        return pltpu.make_async_remote_copy(
+            src_ref=out_x.at[j, part_rows(j, p)],
+            dst_ref=relay_x.at[j, part_rows(j, p)],
+            send_sem=r_send.at[2 * j + p],
+            recv_sem=r_recv.at[2 * j + p],
+            device_id={"ep": me + quarter},
+            device_id_type=MESH,
+        )
+
+    def pass_on(j, p):
+        count = 2 * sizes[j]
+        relay(j, p).wait_recv()
+
+        def one(k):
+            pltpu.make_async_remote_copy(
+                src_ref=relay_x.at[j, pl.ds(k * count, count)],
+                dst_ref=in_x.at[j, pl.ds((spot - quarter) * count, count)],
+                send_sem=h_send.at[j],
+                recv_sem=d_recv.at[j],
+                device_id={"ep": base + k},
+                device_id_type=MESH,
+            ).start()
+
+        each(p * quarter, (p + 1) * quarter, one)
+
     def keep_dispatch(j):
         count = 2 * sizes[j]
 
@@ -243,14 +283,33 @@
         def _():
             wait(rows_odd)
 
-    def dispatched(j, sent):
+    def dispatched(j):
         count = 2 * sizes[j]
-
-        def wait(rows):
-            copy = rows_copy(out_x, in_x, j, rows, d_send, d_recv)
-            copy.wait_send() if sent else copy.wait_recv()
-
-        by_core((side - 1) * count, side * count, wait)
+        by_core(
+            (side - 1) * count,
+            side * count,
+            lambda rows: rows_copy(out_x, in_x, j, rows, d_send, d_recv).wait_recv(),
+        )
+
+    def dispatch_left(j):
+        count = 2 * sizes[j]
+
+        @pl.when(core == 0)
+        def _():
+            rows_copy(out_x, in_x, j, (side - 1) * count, d_send, d_recv).wait_send()
+
+        @pl.when(core - role[0] == 1)
+        def _():
+            rows_copy(out_x, in_x, j, side * count, d_send, d_recv).wait_send()
+
+        @pl.when(role[0] == 1)
+        def _():
+            for p in range(2):
+                relay(j, p).wait_send()
+
+        @pl.when(role[1] == 1)
+        def _():
+            rows_copy(relay_x, in_x, j, side * count, h_send, d_recv).wait_send()
 
     def returned(j, sent):
         def wait(rows):
@@ -275,7 +334,7 @@
     def give_back(j):
         size = sizes[j]
 
-        first = near_first * spot + core * (1 - upper) * quarter
+        first = near_first * spot + (role[0] + role[1]) * quarter
 
         def one(i):
             k = lax.rem(first + i, side)
@@ -306,7 +365,7 @@
 
     def arrive(j):
         with phase(f"arrive{j}"):
-            dispatched(j, False)
+            dispatched(j)
             forward(j).start()
 
     def to_cols(ref, j, at):
@@ -371,21 +430,19 @@
 
             with phase("enter"):
 
-                @pl.when(last_far == 0)
+                @pl.when(role[3] == 0)
                 def _():
-                    entered = side * (1 - lower_far) + (1 + quarter) * lower_far + core * upper
+                    entered = side * (1 - core) + 2 * role[0]
+                    entered = entered + (1 + quarter) * role[1] + (1 + side) * role[2]
                     pl.semaphore_wait(barrier, entered)
 
-        dispatch(j, near_first, side - quarter * lower_far)
+        dispatch(j, near_first, side * (1 - role[0]) - quarter * role[1])
         keep_dispatch(j)
 
-    with phase("ready"):
-
-        @pl.when(lower_far == 1)
-        def _():
-            pl.semaphore_wait(ready, quarter)
-            for j in chunks:
-                dispatch(j, quarter, side)
+        @pl.when(role[0] == 1)
+        def _():
+            relay(j, 1).start()
+            relay(j, 0).start()
 
     small[2].wait()
     mine = (picked - core * half_rows).T
@@ -406,29 +463,49 @@
     spread[half_rows:, :] = turned - high.astype(f32)
     x_cols[...] = jnp.zeros(x_cols.shape, bf16)
 
+    with phase("ready"):
+
+        @pl.when(role[1] == 1)
+        def _():
+            pl.semaphore_wait(ready, quarter)
+            dispatch(0, quarter, side)
+            pass_on(0, 1)
+            pass_on(0, 0)
+            for j in chunks[1:]:
+                dispatch(j, quarter, side)
+
     arrive(0)
+    with phase("pass"):
+
+        @pl.when(role[1] == 1)
+        def _():
+            for j in chunks[1:]:
+                pass_on(j, 1)
+                pass_on(j, 0)
+
     for load in loads[:2]:
         load.wait()
+    last = len(sizes) - 1
+    late = upper * (1 - core)
+    soon = upper * core
     for j in chunks:
         with phase(f"cols{j}"):
             to_cols(in_x, j, 0)
+        if j > 0:
+
+            @pl.when(late == 0)
+            def _():
+                finish(j - 1)
+
         with phase(f"forward{j}"):
             forward(j).wait_recv()
-        if j + 1 < len(sizes):
-
-            @pl.when(core == 0)
-            def _():
-                arrive(j + 1)
-
         with phase(f"sib{j}"):
             to_cols(sib_x, j, pad)
         with phase(f"project{j}"):
             project(j)
-        if j > 0:
-            finish(j - 1)
-        if j + 1 < len(sizes):
-
-            @pl.when(core == 1)
+        if j < last:
+
+            @pl.when(soon == 1)
             def _():
                 arrive(j + 1)
 
@@ -436,9 +513,33 @@
             loads[2].wait()
         with phase(f"down{j}"):
             down(j)
-    finish(len(sizes) - 1)
+        if j < last:
+
+            @pl.when(soon == 0)
+            def _():
+                arrive(j + 1)
+
+        if j > 0:
+
+            @pl.when(late == 1)
+            def _():
+                finish(j - 1)
+
+    with phase("left"):
+        for j in chunks:
+            dispatch_left(j)
+            forward(j).wait_send()
+    finish(last)
+    with phase("left"):
+        for j in chunks:
+            for k in range(CUTS):
+                swap(j, k).wait_send()
+        for j in chunks[:last]:
+            returned(j, True)
 
     for j in chunks:
+        if j == last:
+            returned(j, True)
         with phase(f"returned{j}"):
             returned(j, False)
         block = 8 * sizes[j]
@@ -459,13 +560,6 @@
         res = r_cols[:, part].astype(bf16)
         total = jnp.dot(spread[...].astype(bf16), res, preferred_element_type=f32)
         mixed[:, part] = (total[:half_rows] + total[half_rows:]).astype(bf16)
-
-    for j in chunks:
-        dispatched(j, True)
-        forward(j).wait_send()
-        for k in range(CUTS):
-            swap(j, k).wait_send()
-        returned(j, True)
 
 
 def local(n, tokens, norm_gain, chosen_rows, route_weights, gate_weight, up_weight, down_weight):
@@ -499,6 +593,7 @@
         packed,
         packed,
         packed,
+        packed,
         pltpu.VMEM((max(block, 8 * top) * pieces, LANES), f32),
         pltpu.VMEM((blocks, 2 * pad, width), bf16),
         pltpu.VMEM((blocks, 2 * pad, ff), bf16),
@@ -519,8 +614,9 @@
         in_specs=[hbm] * 7,
         out_specs=vmem,
         scratch_shapes=scratch
-        + [pltpu.SemaphoreType.DMA((7,))]
-        + [pltpu.SemaphoreType.DMA((CUTS * parts,))] * 8
+        + [pltpu.SemaphoreType.DMA((parts,))] * 8
+        + [pltpu.SemaphoreType.DMA((2 * parts,))] * 2
+        + [pltpu.SemaphoreType.DMA((parts,))]
         + [pltpu.SemaphoreType.REGULAR],
         compiler_params=pltpu.CompilerParams(
             collective_id=0, has_side_effects=True, vmem_limit_bytes=limit

time: 22.7 us -> 22.8 us (level)
  no operation moved by 1% of the time
where the time goes in v2:
time: 22.8 us; the launch traced here: 22.7 us
  Pallas kernels  22 us (96%)
  local copies, waits for them, and re-layouts  0.72 us (3%)
    pallas_call x1, Pallas kernels, local(): pl.pallas_call(functools.partial(kernel, n), out_shape=pltpu.VMEM((half_r...  22 us
    unnamed x1, local copies, waits for them, and re-layouts  0.72 us

profile of v2, /device:TPU:0, one launch (start us, length us, event | category | flops | bytes accessed | tf_op | source)
XLA Modules:
  0.0 22.7 jit_solution(11711292471478632854)
XLA Ops:
  0.0 22.0 %shard_map.73 = bf16[72,2048]{1,0:T(8,128)(2,1)S(1)} custom-call(bf16[144,2048]{1,0:T(8,128)(2,1)} %tokens.1, bf16[2048]{0:T(1024)(128)(2,1)} %gain_h.1, s32[8,18]{1,0:T(8,128)} %chosen_h.1, f32[8,18]{1,0:T(8,128)} %route_h.1, bf16[1,2048,768]{2,1,0:T(8,128)(2,1)} %gate_w.1, bf16[1,2048,768]{2,1,0:T(8,128)(2,1)} %up_w.1, bf16[1,768,2048]{2,1,0:T(8,128)(2,1)} %down_w.1), custom_call_target="tpu_custom_call" | custom-call | tf_op jit(solution)/shard_map/pallas_call | solution.py:611
  22.0 0.7 %copy.9 = bf16[72,2048]{1,0:T(8,128)(2,1)} copy(bf16[72,2048]{1,0:T(8,128)(2,1)S(1)} %shard_map.73) | data formatting | bytes 589824

commit v3 on v2

--- a/solution.py
+++ b/solution.py
@@ -10,7 +10,6 @@
 MESH = pl.DeviceIdType.MESH
 LANES = 128
 PARTS = 2
-CUTS = 1
 TILE = 256
 VMEM_BYTES = 67043328
 
@@ -57,14 +56,11 @@
     wd,
     out_x,
     in_x,
-    sib_x,
     relay_x,
     flat,
     x_cols,
-    hidden,
-    p_send,
+    sums,
     p_recv,
-    p_own,
     c_send,
     c_recv,
     g_rows,
@@ -95,9 +91,10 @@
     quarter = n // 4
     bunch = min(side, 4)
     blocks = side // bunch
-    pad = x_cols.shape[1] // 2
+    pad = round_up(bunch * 2 * max(sizes), 16)
+    first_pad = round_up(bunch * 2 * sizes[0], 16)
     pieces = width // LANES
-    cols = width // CUTS
+    cols = width // 2
     f32, bf16 = jnp.float32, jnp.bfloat16
     me = lax.axis_index("ep")
     core = lax.axis_index("tp")
@@ -115,11 +112,11 @@
         pl.semaphore_signal(semaphore, inc=1, device_id=target, device_id_type=MESH)
 
     greet(barrier, sib)
-    near_first = 1 - core
+    even = 1 - core
     each(
-        near_first + quarter * role[2],
+        even + quarter * role[2],
         side * (1 - role[3]),
-        lambda i: greet(barrier, {"ep": base + lax.rem(spot * near_first + i, side)}),
+        lambda i: greet(barrier, {"ep": base + lax.rem(spot * even + i, side)}),
     )
 
     @pl.when(role[1] == 1)
@@ -214,10 +211,10 @@
         count = 2 * sizes[j]
 
         def one(i):
-            k = lax.rem(spot * near_first + i, side)
+            k = lax.rem(spot * even + i, side)
             pltpu.make_async_remote_copy(
                 src_ref=out_x.at[j, pl.ds(k * count, count)],
-                dst_ref=in_x.at[j, pl.ds(spot * count, count)],
+                dst_ref=in_x.at[2 * core + j, pl.ds(spot * count, count)],
                 send_sem=d_send.at[j],
                 recv_sem=d_recv.at[j],
                 device_id={"ep": base + k},
@@ -247,7 +244,7 @@
         def one(k):
             pltpu.make_async_remote_copy(
                 src_ref=relay_x.at[j, pl.ds(k * count, count)],
-                dst_ref=in_x.at[j, pl.ds((spot - quarter) * count, count)],
+                dst_ref=in_x.at[2 + j, pl.ds((spot - quarter) * count, count)],
                 send_sem=h_send.at[j],
                 recv_sem=d_recv.at[j],
                 device_id={"ep": base + k},
@@ -319,22 +316,36 @@
         by_core((n - 1) * sizes[j], n * sizes[j], wait)
 
     def forward(j):
-        return rows_copy(in_x, sib_x, j, side * 2 * sizes[j], f_send, f_recv)
-
-    def swap(j, k):
+        rows = pl.ds(0, side * 2 * sizes[j])
         return pltpu.make_async_remote_copy(
-            src_ref=p_send.at[j, k],
-            dst_ref=p_recv.at[j, k],
-            send_sem=q_send.at[CUTS * j + k],
-            recv_sem=q_recv.at[CUTS * j + k],
+            src_ref=in_x.at[2 * core + j, rows],
+            dst_ref=in_x.at[2 * core + j, rows],
+            send_sem=f_send.at[j],
+            recv_sem=f_recv.at[j],
             device_id=sib,
             device_id_type=MESH,
         )
 
+    def even_sum(j):
+        return 4 * upper if j == 0 else 1
+
+    def own_sum(j):
+        return core * (2 + j) + (1 - core) * even_sum(j)
+
+    def swap(j):
+        return pltpu.make_async_remote_copy(
+            src_ref=sums.at[(1 - core) * (2 + j) + core * even_sum(j)],
+            dst_ref=p_recv.at[j],
+            send_sem=q_send.at[j],
+            recv_sem=q_recv.at[j],
+            device_id=sib,
+            device_id_type=MESH,
+        )
+
     def give_back(j):
         size = sizes[j]
 
-        first = near_first * spot + (role[0] + role[1]) * quarter
+        first = even * spot + (role[0] + role[1]) * quarter
 
         def one(i):
             k = lax.rem(first + i, side)
@@ -348,7 +359,7 @@
                     device_id_type=MESH,
                 ).start()
 
-        each(near_first, side, one)
+        each(even, side, one)
 
         @pl.when(core == 0)
         def _():
@@ -368,11 +379,15 @@
             dispatched(j)
             forward(j).start()
 
-    def to_cols(ref, j, at):
+    windows = [0, pad, pad + first_pad]
+
+    def to_cols(index):
+        j = index % 2
         count = bunch * 2 * sizes[j]
+        at = windows[0 if index > 1 else 1 + j]
 
         def one(b):
-            got = ref[j, block_rows(b, count)].astype(f32)
+            got = in_x[index, block_rows(b, count)].astype(f32)
             flat[pl.ds(0, count * pieces), :] = got.reshape(count * pieces, LANES)
             for s in range(pieces):
                 x_cols[b, at : at + count, s * LANES : (s + 1) * LANES] = flat[
@@ -381,44 +396,43 @@
 
         loop(blocks, one)
 
-    def project(j):
+    def experts_part(j):
+        tiles = range(0, ff, TILE)
+
         def one(b):
-            for c in range(0, ff, TILE):
+            def both(c):
                 gate = jnp.dot(x_cols[b], wgu[:, c : c + TILE], preferred_element_type=f32)
                 up = jnp.dot(x_cols[b], wgu[:, ff + c : ff + c + TILE], preferred_element_type=f32)
-                hidden[b, :, c : c + TILE] = (gate / (1.0 + jnp.exp(-gate)) * up).astype(bf16)
+                return gate, up
+
+            total = None
+            ahead = both(0)
+            for c in tiles:
+                gate, up = ahead
+                if c + TILE < ff:
+                    ahead = both(c + TILE)
+                act = (gate / (1.0 + jnp.exp(-gate)) * up).astype(bf16)
+                got = jnp.dot(act, wd[c : c + TILE, :], preferred_element_type=f32)
+                total = got if total is None else total + got
+            for window, k, index in ((0, j, 2 + j), (1, 0, 4 * j), (2, 1, 1)):
+                if k <= j:
+                    at, count = windows[window], bunch * 2 * sizes[k]
+                    sums[index, b, :count] = total[at : at + count].astype(bf16)
 
         loop(blocks, one)
-
-    def down(j):
-        count = bunch * 2 * sizes[j]
-        for k in range(CUTS):
-            part = slice(k * cols, (k + 1) * cols)
-
-            def one(b):
-                got = jnp.dot(hidden[b], wd[:, part], preferred_element_type=f32)
-                p_send[j, k, b, :count] = got[pad : pad + count].astype(bf16)
-                p_own[j, k, b, :count] = got[:count].astype(bf16)
-
-            loop(blocks, one)
-            swap(j, k).start()
 
     def combine(j):
         count = bunch * 2 * sizes[j]
 
         def one(b):
-            both = [
-                p_own[j, k, b, :count].astype(f32) + p_recv[j, k, b, :count].astype(f32)
-                for k in range(CUTS)
-            ]
-            pack(jnp.concatenate(both, axis=1), c_send, j, b)
+            both = sums[own_sum(j), b, :count].astype(f32) + p_recv[j, b, :count].astype(f32)
+            pack(both, c_send, j, b)
 
         loop(blocks, one)
 
     def finish(j):
         with phase(f"swap{j}"):
-            for k in range(CUTS):
-                swap(j, k).wait_recv()
+            swap(j).wait_recv()
         with phase(f"combine{j}"):
             combine(j)
             give_back(j)
@@ -436,13 +450,13 @@
                     entered = entered + (1 + quarter) * role[1] + (1 + side) * role[2]
                     pl.semaphore_wait(barrier, entered)
 
-        dispatch(j, near_first, side * (1 - role[0]) - quarter * role[1])
+        dispatch(j, even, side * (1 - role[0]) - quarter * role[1])
         keep_dispatch(j)
 
         @pl.when(role[0] == 1)
         def _():
-            relay(j, 1).start()
-            relay(j, 0).start()
+            for p in (0, 1) if j == 0 else (1, 0):
+                relay(j, p).start()
 
     small[2].wait()
     mine = (picked - core * half_rows).T
@@ -467,10 +481,10 @@
 
         @pl.when(role[1] == 1)
         def _():
+            pass_on(0, 0)
             pl.semaphore_wait(ready, quarter)
             dispatch(0, quarter, side)
             pass_on(0, 1)
-            pass_on(0, 0)
             for j in chunks[1:]:
                 dispatch(j, quarter, side)
 
@@ -485,45 +499,45 @@
 
     for load in loads[:2]:
         load.wait()
-    last = len(sizes) - 1
-    late = upper * (1 - core)
-    soon = upper * core
-    for j in chunks:
-        with phase(f"cols{j}"):
-            to_cols(in_x, j, 0)
-        if j > 0:
-
-            @pl.when(late == 0)
-            def _():
-                finish(j - 1)
-
+    last = 1
+    lower = 1 - upper
+    odd = core
+
+    def when(flag, *steps):
+        @pl.when(flag == 1)
+        def _():
+            for step, *args in steps:
+                step(*args)
+
+    def came(j):
         with phase(f"forward{j}"):
             forward(j).wait_recv()
-        with phase(f"sib{j}"):
-            to_cols(sib_x, j, pad)
-        with phase(f"project{j}"):
-            project(j)
-        if j < last:
-
-            @pl.when(soon == 1)
-            def _():
-                arrive(j + 1)
-
-        if j == 0:
-            loads[2].wait()
-        with phase(f"down{j}"):
-            down(j)
-        if j < last:
-
-            @pl.when(soon == 0)
-            def _():
-                arrive(j + 1)
-
-        if j > 0:
-
-            @pl.when(late == 1)
-            def _():
-                finish(j - 1)
+
+    def send(j):
+        swap(j).start()
+
+    when(odd, (to_cols, 2))
+    when(odd * lower, (came, 0))
+    when(lower, (to_cols, 0))
+    when(even, (came, 0), (to_cols, 2))
+    loads[2].wait()
+    with phase("down0"):
+        experts_part(0)
+    when(1 - odd * upper, (send, 0))
+    arrive(1)
+    when(odd, (to_cols, 3))
+    when(even, (to_cols, 1))
+    when(1 - even * upper, (finish, 0))
+    when(odd * upper, (came, 0))
+    when(upper, (to_cols, 0))
+    came(1)
+    when(odd, (to_cols, 1))
+    when(even, (to_cols, 3))
+    with phase("down1"):
+        experts_part(1)
+    when(odd * upper, (send, 0))
+    send(1)
+    when(even * upper, (finish, 0))
 
     with phase("left"):
         for j in chunks:
@@ -532,8 +546,7 @@
     finish(last)
     with phase("left"):
         for j in chunks:
-            for k in range(CUTS):
-                swap(j, k).wait_send()
+            swap(j).wait_send()
         for j in chunks[:last]:
             returned(j, True)
 
@@ -555,7 +568,7 @@
                 ]
 
         loop(experts // 8, unpack)
-    for k in range(CUTS):
+    for k in range(2):
         part = slice(k * cols, (k + 1) * cols)
         res = r_cols[:, part].astype(bf16)
         total = jnp.dot(spread[...].astype(bf16), res, preferred_element_type=f32)
@@ -576,11 +589,11 @@
     blocks = side // bunch
     block = bunch * 2 * top
     pad = round_up(block, 16)
+    first_pad = round_up(bunch * 2 * sizes[0], 16)
     pieces = width // LANES
     ff = gate_weight.shape[2]
     bf16, f32 = jnp.bfloat16, jnp.float32
     packed = pltpu.VMEM((parts, n * top, pieces, LANES), bf16)
-    partial = pltpu.VMEM((parts, CUTS, blocks, block, width // CUTS), bf16)
     vmem = pl.BlockSpec(memory_space=pltpu.VMEM)
     hbm = pl.BlockSpec(memory_space=pltpu.HBM)
     scratch = [
@@ -591,15 +604,12 @@
         pltpu.VMEM((width, 2 * ff), bf16),
         pltpu.VMEM(down_weight.shape[1:], bf16),
         packed,
-        packed,
-        packed,
+        pltpu.VMEM((4, n * top, pieces, LANES), bf16),
         packed,
         pltpu.VMEM((max(block, 8 * top) * pieces, LANES), f32),
-        pltpu.VMEM((blocks, 2 * pad, width), bf16),
-        pltpu.VMEM((blocks, 2 * pad, ff), bf16),
-        partial,
-        partial,
-        partial,
+        pltpu.VMEM((blocks, 2 * pad + first_pad, width), bf16),
+        pltpu.VMEM((5, blocks, block, width), bf16),
+        pltpu.VMEM((2, blocks, block, width), bf16),
         packed,
         packed,
         pltpu.VMEM((n * top, tok_rows), f32),

time: 22.8 us -> 22 us (0.965)
  Pallas kernels: 22 us -> 21.1 us
    pallas_call x1, Pallas kernels: 22 us -> 21.1 us  [local(): pl.pallas_call(functools.partial(kernel, n), out_shape=pltpu.VMEM((half_r...]
where the time goes in v3:
time: 22 us; the launch traced here: 21.8 us
  Pallas kernels  21.1 us (96%)
  local copies, waits for them, and re-layouts  0.72 us (3%)
    pallas_call x1, Pallas kernels, local(): pl.pallas_call(functools.partial(kernel, n), out_shape=pltpu.VMEM((half_r...  21.1 us
    unnamed x1, local copies, waits for them, and re-layouts  0.72 us

profile of v3, /device:TPU:0, one launch (start us, length us, event | category | flops | bytes accessed | tf_op | source)
XLA Modules:
  0.0 21.8 jit_solution(6077193352906073179)
XLA Ops:
  0.0 21.1 %shard_map.73 = bf16[72,2048]{1,0:T(8,128)(2,1)S(1)} custom-call(bf16[144,2048]{1,0:T(8,128)(2,1)} %tokens.1, bf16[2048]{0:T(1024)(128)(2,1)} %gain_h.1, s32[8,18]{1,0:T(8,128)} %chosen_h.1, f32[8,18]{1,0:T(8,128)} %route_h.1, bf16[1,2048,768]{2,1,0:T(8,128)(2,1)} %gate_w.1, bf16[1,2048,768]{2,1,0:T(8,128)(2,1)} %up_w.1, bf16[1,768,2048]{2,1,0:T(8,128)(2,1)} %down_w.1), custom_call_target="tpu_custom_call" | custom-call | tf_op jit(solution)/shard_map/pallas_call | solution.py:621
  21.1 0.7 %copy.9 = bf16[72,2048]{1,0:T(8,128)(2,1)} copy(bf16[72,2048]{1,0:T(8,128)(2,1)S(1)} %shard_map.73) | data formatting | bytes 589824

commit v4 on v3

--- a/solution.py
+++ b/solution.py
@@ -65,7 +65,10 @@
     c_recv,
     g_rows,
     w_rows,
-    spread,
+    pair_rows,
+    spread_a,
+    spread_b,
+    held,
     r_cols,
     d_send,
     d_recv,
@@ -95,6 +98,9 @@
     first_pad = round_up(bunch * 2 * sizes[0], 16)
     pieces = width // LANES
     cols = width // 2
+    spread = [spread_a, spread_b]
+    packed_rows = [round_up(experts * size, 16) for size in sizes]
+    packed_at = [0, packed_rows[0]]
     f32, bf16 = jnp.float32, jnp.bfloat16
     me = lax.axis_index("ep")
     core = lax.axis_index("tp")
@@ -123,13 +129,13 @@
     def _():
         greet(barrier, {"ep": me - quarter})
 
-    load_tok = pltpu.make_async_copy(tokens, tok, h_send.at[0])
+    load_tok = pltpu.make_async_copy(tokens, tok, h_send)
     small = [
         pltpu.make_async_copy(src, dst, sem)
         for src, dst, sem in (
-            (gain_h, gain, h_send.at[1]),
-            (chosen_h, chosen, b_send.at[1]),
-            (route_h, route, f_send.at[0]),
+            (gain_h, gain, r_send),
+            (chosen_h, chosen, d_send),
+            (route_h, route, b_send.at[1]),
         )
     ]
     small[1].start()
@@ -140,8 +146,8 @@
     loads = [
         pltpu.make_async_copy(src.at[0], dst, sem)
         for src, dst, sem in (
-            (gate_w, wgu.at[:, pl.ds(0, ff)], q_send.at[0]),
-            (up_w, wgu.at[:, pl.ds(ff, ff)], q_send.at[1]),
+            (gate_w, wgu.at[:, pl.ds(0, ff)], q_send),
+            (up_w, wgu.at[:, pl.ds(ff, ff)], f_send),
             (down_w, wd, b_send.at[0]),
         )
     ]
@@ -215,7 +221,7 @@
             pltpu.make_async_remote_copy(
                 src_ref=out_x.at[j, pl.ds(k * count, count)],
                 dst_ref=in_x.at[2 * core + j, pl.ds(spot * count, count)],
-                send_sem=d_send.at[j],
+                send_sem=d_send,
                 recv_sem=d_recv.at[j],
                 device_id={"ep": base + k},
                 device_id_type=MESH,
@@ -231,7 +237,7 @@
         return pltpu.make_async_remote_copy(
             src_ref=out_x.at[j, part_rows(j, p)],
             dst_ref=relay_x.at[j, part_rows(j, p)],
-            send_sem=r_send.at[2 * j + p],
+            send_sem=r_send,
             recv_sem=r_recv.at[2 * j + p],
             device_id={"ep": me + quarter},
             device_id_type=MESH,
@@ -245,7 +251,7 @@
             pltpu.make_async_remote_copy(
                 src_ref=relay_x.at[j, pl.ds(k * count, count)],
                 dst_ref=in_x.at[2 + j, pl.ds((spot - quarter) * count, count)],
-                send_sem=h_send.at[j],
+                send_sem=h_send,
                 recv_sem=d_recv.at[j],
                 device_id={"ep": base + k},
                 device_id_type=MESH,
@@ -265,8 +271,8 @@
         return pltpu.make_async_remote_copy(
             src_ref=src.at[j, pl.ds(0, rows)],
             dst_ref=dst.at[j, pl.ds(0, rows)],
-            send_sem=send_sem.at[j],
-            recv_sem=recv_sem.at[j],
+            send_sem=send_sem,
+            recv_sem=recv_sem,
             device_id=sib,
             device_id_type=MESH,
         )
@@ -285,33 +291,43 @@
         by_core(
             (side - 1) * count,
             side * count,
-            lambda rows: rows_copy(out_x, in_x, j, rows, d_send, d_recv).wait_recv(),
+            lambda rows: rows_copy(out_x, in_x, j, rows, d_send, d_recv.at[j]).wait_recv(),
         )
 
-    def dispatch_left(j):
-        count = 2 * sizes[j]
-
+    def both_chunks(ref, rows):
+        return ref.at[pl.ds(0, 2), pl.ds(0, rows)]
+
+    def sent(ref, semaphore):
+        pltpu.make_async_remote_copy(
+            src_ref=ref,
+            dst_ref=ref,
+            send_sem=semaphore,
+            recv_sem=d_recv.at[0],
+            device_id=sib,
+            device_id_type=MESH,
+        ).wait_send()
+
+    def dispatch_left():
         @pl.when(core == 0)
         def _():
-            rows_copy(out_x, in_x, j, (side - 1) * count, d_send, d_recv).wait_send()
+            sent(both_chunks(out_x, (side - 1) * half), d_send)
 
         @pl.when(core - role[0] == 1)
         def _():
-            rows_copy(out_x, in_x, j, side * count, d_send, d_recv).wait_send()
+            sent(both_chunks(out_x, side * half), d_send)
 
         @pl.when(role[0] == 1)
         def _():
-            for p in range(2):
-                relay(j, p).wait_send()
+            sent(both_chunks(out_x, side * half), r_send)
 
         @pl.when(role[1] == 1)
         def _():
-            rows_copy(relay_x, in_x, j, side * count, h_send, d_recv).wait_send()
-
-    def returned(j, sent):
+            sent(both_chunks(relay_x, side * half), h_send)
+
+    def returned(j, left):
         def wait(rows):
-            copy = rows_copy(c_recv, c_recv, j, rows, b_send, b_recv)
-            copy.wait_send() if sent else copy.wait_recv()
+            copy = rows_copy(c_recv, c_recv, j, rows, b_send.at[j], b_recv.at[j])
+            copy.wait_send() if left else copy.wait_recv()
 
         by_core((n - 1) * sizes[j], n * sizes[j], wait)
 
@@ -320,7 +336,7 @@
         return pltpu.make_async_remote_copy(
             src_ref=in_x.at[2 * core + j, rows],
             dst_ref=in_x.at[2 * core + j, rows],
-            send_sem=f_send.at[j],
+            send_sem=f_send,
             recv_sem=f_recv.at[j],
             device_id=sib,
             device_id_type=MESH,
@@ -336,7 +352,7 @@
         return pltpu.make_async_remote_copy(
             src_ref=sums.at[(1 - core) * (2 + j) + core * even_sum(j)],
             dst_ref=p_recv.at[j],
-            send_sem=q_send.at[j],
+            send_sem=q_send,
             recv_sem=q_recv.at[j],
             device_id=sib,
             device_id_type=MESH,
@@ -455,13 +471,15 @@
 
         @pl.when(role[0] == 1)
         def _():
-            for p in (0, 1) if j == 0 else (1, 0):
+            for p in (0, 1):
                 relay(j, p).start()
 
     small[2].wait()
     mine = (picked - core * half_rows).T
     weight = route[...].T
     lane = lax.broadcasted_iota(jnp.int32, (half, half_rows), 1).astype(f32)
+    w_rows[...] = jnp.zeros(w_rows.shape, f32)
+    r_cols[...] = jnp.zeros(r_cols.shape, f32)
     for e in range(experts):
         pair = [mine[h * half : (h + 1) * half, e : e + 1] for h in range(2)]
         row = jnp.where(core == 0, pair[0], pair[1])
@@ -469,12 +487,15 @@
         share = jnp.where(core == 0, pair[0], pair[1])
         here = jnp.where(lane == row, share, 0.0)
         for j, size in enumerate(sizes):
-            at = experts * starts[j] + e * size
+            at = packed_at[j] + e * size
             w_rows[at : at + size, :] = here[starts[j] : starts[j] + size]
-    turned = w_rows[...].T
-    high = turned.astype(bf16)
-    spread[:half_rows, :] = high.astype(f32)
-    spread[half_rows:, :] = turned - high.astype(f32)
+    for j in chunks:
+        some = packed_rows[j]
+        value = w_rows[packed_at[j] : packed_at[j] + some, :]
+        high = value.astype(bf16).astype(f32)
+        pair_rows[:some, :] = high
+        pair_rows[some : 2 * some, :] = value - high
+        spread[j][...] = pair_rows[: 2 * some, :].T
     x_cols[...] = jnp.zeros(x_cols.shape, bf16)
 
     with phase("ready"):
@@ -487,7 +508,10 @@
             pass_on(0, 1)
             for j in chunks[1:]:
                 dispatch(j, quarter, side)
-
+                pass_on(j, 0)
+
+    for load in loads[:2]:
+        load.wait()
     arrive(0)
     with phase("pass"):
 
@@ -495,10 +519,7 @@
         def _():
             for j in chunks[1:]:
                 pass_on(j, 1)
-                pass_on(j, 0)
-
-    for load in loads[:2]:
-        load.wait()
+
     last = 1
     lower = 1 - upper
     odd = core
@@ -540,15 +561,12 @@
     when(even * upper, (finish, 0))
 
     with phase("left"):
-        for j in chunks:
-            dispatch_left(j)
-            forward(j).wait_send()
+        dispatch_left()
+        sent(both_chunks(in_x, side * half), f_send)
     finish(last)
     with phase("left"):
-        for j in chunks:
-            swap(j).wait_send()
-        for j in chunks[:last]:
-            returned(j, True)
+        sent(sums.at[pl.ds(0, 2)], q_send)
+        returned(0, True)
 
     for j in chunks:
         if j == last:
@@ -560,7 +578,7 @@
         def unpack(b):
             got = c_recv[j, block_rows(b, block)].astype(f32)
             flat[: block * pieces, :] = got.reshape(block * pieces, LANES)
-            at = experts * starts[j] + b * block
+            at = packed_at[j] + b * block
             at = at if isinstance(b, int) else pl.multiple_of(at, 8)
             for s in range(pieces):
                 r_cols[pl.ds(at, block), s * LANES : (s + 1) * LANES] = flat[
@@ -568,11 +586,16 @@
                 ]
 
         loop(experts // 8, unpack)
-    for k in range(2):
-        part = slice(k * cols, (k + 1) * cols)
-        res = r_cols[:, part].astype(bf16)
-        total = jnp.dot(spread[...].astype(bf16), res, preferred_element_type=f32)
-        mixed[:, part] = (total[:half_rows] + total[half_rows:]).astype(bf16)
+        here = slice(packed_at[j], packed_at[j] + packed_rows[j])
+        for k in range(2):
+            part = slice(k * cols, (k + 1) * cols)
+            res = r_cols[here, part].astype(bf16)
+            twice = jnp.concatenate([res, res], axis=0)
+            total = jnp.dot(spread[j][...].astype(bf16), twice, preferred_element_type=f32)
+            if j == 0:
+                held[:, part] = total
+            else:
+                mixed[:, part] = (held[:, part] + total).astype(bf16)
 
 
 def local(n, tokens, norm_gain, chosen_rows, route_weights, gate_weight, up_weight, down_weight):
@@ -580,8 +603,8 @@
     half_rows = tok_rows // 2
     experts, slots = chosen_rows.shape
     half = slots // 2
-    rows = experts * half
     sizes = group_sizes(half)
+    packed_rows = [round_up(experts * size, 16) for size in sizes]
     parts = len(sizes)
     top = max(sizes)
     side = n // 2
@@ -613,9 +636,12 @@
         packed,
         packed,
         pltpu.VMEM((n * top, tok_rows), f32),
-        pltpu.VMEM((rows, half_rows), f32),
-        pltpu.VMEM((tok_rows, rows), f32),
-        pltpu.VMEM((rows, width), f32),
+        pltpu.VMEM((sum(packed_rows), half_rows), f32),
+        pltpu.VMEM((2 * max(packed_rows), half_rows), f32),
+        pltpu.VMEM((half_rows, 2 * packed_rows[0]), f32),
+        pltpu.VMEM((half_rows, 2 * packed_rows[1]), f32),
+        pltpu.VMEM((half_rows, width), f32),
+        pltpu.VMEM((sum(packed_rows), width), f32),
     ]
     limit = VMEM_BYTES - half_rows * width * 2
     return pl.pallas_call(
@@ -624,9 +650,9 @@
         in_specs=[hbm] * 7,
         out_specs=vmem,
         scratch_shapes=scratch
-        + [pltpu.SemaphoreType.DMA((parts,))] * 8
-        + [pltpu.SemaphoreType.DMA((2 * parts,))] * 2
-        + [pltpu.SemaphoreType.DMA((parts,))]
+        + [pltpu.SemaphoreType.DMA, pltpu.SemaphoreType.DMA((parts,))] * 3
+        + [pltpu.SemaphoreType.DMA((parts,))] * 2
+        + [pltpu.SemaphoreType.DMA, pltpu.SemaphoreType.DMA((2 * parts,)), pltpu.SemaphoreType.DMA]
         + [pltpu.SemaphoreType.REGULAR],
         compiler_params=pltpu.CompilerParams(
             collective_id=0, has_side_effects=True, vmem_limit_bytes=limit

time: 22 us -> 21.9 us (level)
  no operation moved by 1% of the time
where the time goes in v4:
time: 21.9 us; the launch traced here: 21.8 us
  Pallas kernels  21 us (96%)
  local copies, waits for them, and re-layouts  0.72 us (3%)
    pallas_call x1, Pallas kernels, local(): pl.pallas_call(functools.partial(kernel, n), out_shape=pltpu.VMEM((half_r...  21 us
    unnamed x1, local copies, waits for them, and re-layouts  0.72 us

profile of v4, /device:TPU:0, one launch (start us, length us, event | category | flops | bytes accessed | tf_op | source)
XLA Modules:
  0.0 21.8 jit_solution(13524189091519050)
XLA Ops:
  0.0 21.0 %shard_map.73 = bf16[72,2048]{1,0:T(8,128)(2,1)S(1)} custom-call(bf16[144,2048]{1,0:T(8,128)(2,1)} %tokens.1, bf16[2048]{0:T(1024)(128)(2,1)} %gain_h.1, s32[8,18]{1,0:T(8,128)} %chosen_h.1, f32[8,18]{1,0:T(8,128)} %route_h.1, bf16[1,2048,768]{2,1,0:T(8,128)(2,1)} %gate_w.1, bf16[1,2048,768]{2,1,0:T(8,128)(2,1)} %up_w.1, bf16[1,768,2048]{2,1,0:T(8,128)(2,1)} %down_w.1), custom_call_target="tpu_custom_call" | custom-call | tf_op jit(solution)/shard_map/pallas_call | solution.py:647
  21.0 0.7 %copy.9 = bf16[72,2048]{1,0:T(8,128)(2,1)} copy(bf16[72,2048]{1,0:T(8,128)(2,1)S(1)} %shard_map.73) | data formatting | bytes 589824

commit v5 on v4

--- a/solution.py
+++ b/solution.py
@@ -117,13 +117,17 @@
     def greet(semaphore, target):
         pl.semaphore_signal(semaphore, inc=1, device_id=target, device_id_type=MESH)
 
-    greet(barrier, sib)
     even = 1 - core
+    lower_odd = role[0] + role[1]
     each(
         even + quarter * role[2],
         side * (1 - role[3]),
-        lambda i: greet(barrier, {"ep": base + lax.rem(spot * even + i, side)}),
+        lambda i: greet(
+            barrier,
+            {"ep": base + lax.rem(spot * even + i + lower_odd * (side - 1 - 2 * i), side)},
+        ),
     )
+    greet(barrier, sib)
 
     @pl.when(role[1] == 1)
     def _():

time: 21.9 us -> 21.9 us (level)
  no operation moved by 1% of the time
where the time goes in v5:
time: 21.9 us; the launch traced here: 21.8 us
  Pallas kernels  21 us (96%)
  local copies, waits for them, and re-layouts  0.72 us (3%)
    pallas_call x1, Pallas kernels, local(): pl.pallas_call(functools.partial(kernel, n), out_shape=pltpu.VMEM((half_r...  21 us
    unnamed x1, local copies, waits for them, and re-layouts  0.72 us

profile of v5, /device:TPU:0, one launch (start us, length us, event | category | flops | bytes accessed | tf_op | source)
XLA Modules:
  0.0 21.8 jit_solution(11440395003376345499)
XLA Ops:
  0.0 21.0 %shard_map.73 = bf16[72,2048]{1,0:T(8,128)(2,1)S(1)} custom-call(bf16[144,2048]{1,0:T(8,128)(2,1)} %tokens.1, bf16[2048]{0:T(1024)(128)(2,1)} %gain_h.1, s32[8,18]{1,0:T(8,128)} %chosen_h.1, f32[8,18]{1,0:T(8,128)} %route_h.1, bf16[1,2048,768]{2,1,0:T(8,128)(2,1)} %gate_w.1, bf16[1,2048,768]{2,1,0:T(8,128)(2,1)} %up_w.1, bf16[1,768,2048]{2,1,0:T(8,128)(2,1)} %down_w.1), custom_call_target="tpu_custom_call" | custom-call | tf_op jit(solution)/shard_map/pallas_call | solution.py:651
  21.0 0.7 %copy.9 = bf16[72,2048]{1,0:T(8,128)(2,1)} copy(bf16[72,2048]{1,0:T(8,128)(2,1)S(1)} %shard_map.73) | data formatting | bytes 589824
